TPU v7x, 32 devices: a whole 2x2x4 slice. The times are simulated.
32 devices in a mesh: grp: 2 (over y), sp: 8 (over z, core), tp: 2 (over x).
Axes of the slice: x: 2, y: 2, z: 4, core: 2. Of those that a mesh axis runs over, the one named last changes fastest.
Arguments:
- queries: bfloat16 [12288, 1024], P(('grp', 'sp'), 'tp'), parts along dimension 0, may hold values from -200 to 200
- key_rows: bfloat16 [12288, 512], P(('grp', 'sp'), 'tp'), parts along dimension 0, may hold values from -6 to 6
- value_rows: bfloat16 [12288, 512], P(('grp', 'sp'), 'tp'), parts along dimension 0, may hold values from -6 to 6
- doc_ids: int32 [12288], P(('grp', 'sp')), parts along dimension 0, may hold values from 0 to 3, never falling along the last dimension, each value on 1 to 3072 neighbouring positions
- sink_logits: float32 [16], P('tp'), may hold values from 2 to 7
- out_weight: bfloat16 [1024, 2048], P('tp', 'sp'), may hold values from -0.1875 to 0.1875
- residual: bfloat16 [12288, 2048], P(('grp', 'sp', 'tp')), parts along dimension 0, may hold values from -6 to 6
- gain_mixed: float32 [2048], replicated, may hold values from 0.1 to 1.9
- gain_before: float32 [2048], replicated, may hold values from 0.1 to 1.9
- gain_after: float32 [2048], replicated, may hold values from 0.1 to 1.9
- gate_weight: bfloat16 [2048, 6144], P('sp', 'tp'), may hold values from -0.125 to 0.125
- up_weight: bfloat16 [2048, 6144], P('sp', 'tp'), may hold values from -0.125 to 0.125
- down_weight: bfloat16 [6144, 2048], P('tp', 'sp'), may hold values from -0.078125 to 0.078125
Outputs:
- layer_out: bfloat16 [12288, 2048], P(('grp', 'sp', 'tp')), parts along dimension 0
There are 2 independent parts, one for each index of `grp`. A program takes and returns all parts, laid end to end along the dimension named above; an argument that names none is the same for every part. Nothing has to cross between parts.
All inputs are finite; a program needn't handle non-finite values.
Results may differ from a plain program's by a relative error of at most 0.015.
Values may be sent and summed in bfloat16 or wider, within the bound.
No kernel may reach another device: no remote copies, remote signals or barrier semaphores. Data moves between devices by JAX's collectives and lax.ppermute only.
A program may use at most 128 MiB of HBM per device.

v0:
```python
import jax
import jax.numpy as jnp
from jax import lax
from jax.sharding import PartitionSpec as P

HEAD_DIM = 64
WINDOW = 128
epsilon = 1e-06
masked_value = -1e30


def passed_along(value, axis, steps):
    count = lax.axis_size(axis)
    first, last = (max(0, -steps), min(count, count - steps))
    return lax.ppermute(value, axis, [(source, source + steps) for source in range(first, last)])


def stored(value):
    return lax.optimization_barrier(value.astype(jnp.bfloat16)).astype(jnp.float32)


def rms_scaled(value, gain):
    return value * lax.rsqrt(jnp.mean(value * value, axis=-1, keepdims=True) + epsilon) * gain


def windows(array, blocks):
    first = array[:-WINDOW].reshape((blocks, WINDOW) + array.shape[1:])
    second = array[WINDOW:].reshape((blocks, WINDOW) + array.shape[1:])
    return jnp.concatenate([first, second], axis=1)


def attend(queries, key_rows, value_rows, doc_ids, sink_logits):
    length = queries.shape[0]
    blocks = length // WINDOW
    local_kv = key_rows.shape[1] // HEAD_DIM
    group_size = queries.shape[1] // HEAD_DIM // local_kv
    offset = lax.axis_index("sp") * length
    tail_keys, tail_values, tail_docs = passed_along(
        (key_rows[length - WINDOW :], value_rows[length - WINDOW :], doc_ids[length - WINDOW :]),
        "sp",
        1,
    )
    key_blocks = windows(jnp.concatenate([tail_keys, key_rows], axis=0), blocks).reshape(
        blocks, 2 * WINDOW, local_kv, HEAD_DIM
    )
    value_blocks = windows(jnp.concatenate([tail_values, value_rows], axis=0), blocks).reshape(
        blocks, 2 * WINDOW, local_kv, HEAD_DIM
    )
    key_docs = windows(jnp.concatenate([tail_docs, doc_ids], axis=0), blocks)
    key_places = windows(offset - WINDOW + jnp.arange(length + WINDOW, dtype=jnp.int32), blocks)
    query_places = (offset + jnp.arange(length, dtype=jnp.int32)).reshape(blocks, WINDOW)
    query_docs = doc_ids.reshape(blocks, WINDOW)
    query_blocks = queries.reshape(blocks, WINDOW, local_kv, group_size, HEAD_DIM)
    scores = jnp.einsum(
        "bqhgd,bkhd->bhgqk", query_blocks, key_blocks, preferred_element_type=jnp.float32
    ) * HEAD_DIM ** (-0.5)
    distance = query_places[:, :, None] - key_places[:, None, :]
    valid = (distance >= 0) & (distance < WINDOW) & (key_places[:, None, :] >= 0)
    valid = valid & (query_docs[:, :, None] == key_docs[:, None, :])
    scores = jnp.where(valid[:, None, None], scores, masked_value)
    sinks = sink_logits.reshape(local_kv, group_size)[None, :, :, None]
    top = jnp.maximum(jnp.max(scores, axis=-1), sinks)
    weight = jnp.exp(scores - top[..., None])
    denom = jnp.sum(weight, axis=-1) + jnp.exp(sinks - top)
    summed = jnp.einsum(
        "bhgqk,bkhd->bqhgd",
        weight.astype(jnp.bfloat16),
        value_blocks,
        preferred_element_type=jnp.float32,
    )
    scale = jnp.transpose(denom, (0, 3, 1, 2))[..., None]
    return (summed / scale).reshape(length, queries.shape[1]).astype(jnp.bfloat16)


def per_device(
    queries,
    key_rows,
    value_rows,
    doc_ids,
    sink_logits,
    out_weight,
    residual,
    gain_mixed,
    gain_before,
    gain_after,
    gate_weight,
    up_weight,
    down_weight,
):
    mixed = attend(queries, key_rows, value_rows, doc_ids, sink_logits)
    head_columns = lax.all_gather(out_weight, "sp", axis=1, tiled=True)
    projected = lax.psum_scatter(
        jnp.dot(mixed, head_columns, preferred_element_type=jnp.float32).astype(jnp.bfloat16),
        "tp",
        scatter_dimension=0,
        tiled=True,
    ).astype(jnp.float32)
    projected = stored(projected)
    after = stored(residual.astype(jnp.float32) + rms_scaled(projected, gain_mixed))
    normed = rms_scaled(after, gain_before).astype(jnp.bfloat16)
    full_gate, full_up, full_down = (
        lax.all_gather(gate_weight, "sp", axis=0, tiled=True),
        lax.all_gather(up_weight, "sp", axis=0, tiled=True),
        lax.all_gather(down_weight, "sp", axis=1, tiled=True),
    )
    piece = lax.all_gather(normed, "tp", axis=0, tiled=True)
    gate = jnp.dot(piece, full_gate, preferred_element_type=jnp.float32)
    upward = jnp.dot(piece, full_up, preferred_element_type=jnp.float32)
    hidden = (jax.nn.silu(gate) * upward).astype(jnp.bfloat16)
    ffn_out = stored(
        lax.psum_scatter(
            jnp.dot(hidden, full_down, preferred_element_type=jnp.float32).astype(jnp.bfloat16),
            "tp",
            scatter_dimension=0,
            tiled=True,
        ).astype(jnp.float32)
    )
    return (after + 0.5 * rms_scaled(ffn_out, gain_after)).astype(jnp.bfloat16)


def solution(mesh):
    return jax.shard_map(
        per_device,
        mesh=mesh,
        in_specs=(
            P(("grp", "sp"), "tp"),
            P(("grp", "sp"), "tp"),
            P(("grp", "sp"), "tp"),
            P(("grp", "sp")),
            P("tp"),
            P("tp", "sp"),
            P(("grp", "sp", "tp"), None),
            P(),
            P(),
            P(),
            P("sp", "tp"),
            P("sp", "tp"),
            P("tp", "sp"),
        ),
        out_specs=P(("grp", "sp", "tp"), None),
        check_vma=False,
    )
```

profile of v0, /device:TPU:0, one launch (start us, length us, event | category | flops | bytes accessed | tf_op | source)
XLA Modules:
  0.0 577.6 jit_solution(4253527668909372230)
XLA Ops:
  8.0 2.4 collective-permute-start.1
  11.2 5.2 collective-permute-start.2
  17.3 1.3 collective-permute-start
  18.7 1.8 reshape.107
  20.5 1.9 reshape.105
  22.4 1.7 reshape.108
  31.3 2.3 fusion.2
  33.7 1.7 fusion
  35.5 1.6 fusion.20
  37.7 4.6 all-gather.6.cloned.1.call-done
  42.2 5.1 convolution_convert_fusion
  47.4 42.3 %reduce-scatter.3.cloned.1.call-done = bf16[384,2048]{1,0:T(8,128)(2,1)} async-done(((bf16[768,2048]{1,0:T(8,128)(2,1)}), bf16[384,2048]{1,0:T(8,128)(2,1)}) %reduce-scatter.3.cloned.1.call-update) | async-done | bytes 1572880 | tf_op jit(solution)/shard_map/reduce_scatter | solution.py:92
  89.6 1.8 fusion.3
  91.5 2.2 fusion.6
  94.1 1.6 fusion.12
  97.7 43.1 %all-gather.8.cloned.1.call-done = bf16[768,2048]{1,0:T(8,128)(2,1)} async-done(((bf16[384,2048]{1,0:T(8,128)(2,1)}), bf16[768,2048]{1,0:T(8,128)(2,1)}) %all-gather.8.cloned.1.call-update) | async-done | bytes 3145744 | tf_op jit(solution)/shard_map/all_gather | solution.py:106
  140.8 118.2 %all-gather.10.cloned.1.call-done = bf16[2048,3072]{1,0:T(8,128)(2,1)} async-done(((bf16[256,3072]{1,0:T(8,128)(2,1)}), bf16[2048,3072]{1,0:T(8,128)(2,1)}) %all-gather.10.cloned.1.call-update) | async-done | bytes 12582928 | tf_op jit(solution)/shard_map/all_gather | solution.py:102
  259.0 16.0 %fusion.39 = f32[768,3072]{1,0:T(8,128)} fusion(bf16[768,2048]{1,0:T(8,128)(2,1)} %all-gather.8.cloned.1.call-done, bf16[2048,3072]{1,0:T(8,128)(2,1)} %all-gather.10.cloned.1.call-done), kind=kOutput, calls=%fused_computation.67 | convolution fusion | flops 9663676416 | bytes 25165824 | tf_op jit(solution)/shard_map/dot_general | solution.py:107
  275.0 100.4 %all-gather.12.cloned.1.call-done = bf16[2048,3072]{1,0:T(8,128)(2,1)} async-done(((bf16[256,3072]{1,0:T(8,128)(2,1)}), bf16[2048,3072]{1,0:T(8,128)(2,1)}) %all-gather.12.cloned.1.call-update) | async-done | bytes 12582928 | tf_op jit(solution)/shard_map/all_gather | solution.py:103
  375.4 116.8 %all-gather.14.cloned.1.call-done = bf16[3072,2048]{1,0:T(8,128)(2,1)} async-done(((bf16[3072,256]{1,0:T(8,128)(2,1)}), bf16[3072,2048]{1,0:T(8,128)(2,1)}) %all-gather.14.cloned.1.call-update) | async-done | bytes 12582928 | tf_op jit(solution)/shard_map/all_gather | solution.py:104
  492.2 31.5 %convolution_convert_fusion.1 = bf16[768,2048]{1,0:T(8,128)(2,1)} fusion(bf16[3072,2048]{1,0:T(8,128)(2,1)} %all-gather.14.cloned.1.call-done, f32[768,3072]{1,0:T(8,128)} %fusion.39, bf16[768,2048]{1,0:T(8,128)(2,1)} %all-gather.8.cloned.1.call-done, bf16[2048,3072]{1,0:T(8,128)(2,1)} %all-gather.12.cloned.1.call-done), kind=kOutput, calls=%fused_computation.14 | convolution fusion | flops 19343081472 | bytes 40894464 | tf_op jit(solution)/shard_map/dot_general | solution.py:112
  523.8 41.8 %reduce-scatter.5.cloned.1.call-done = bf16[384,2048]{1,0:T(8,128)(2,1)} async-done(((bf16[768,2048]{1,0:T(8,128)(2,1)}), bf16[384,2048]{1,0:T(8,128)(2,1)}) %reduce-scatter.5.cloned.1.call-update) | async-done | bytes 1572880 | tf_op jit(solution)/shard_map/reduce_scatter | solution.py:111
  565.6 1.8 fusion.7
  567.4 3.4 fusion.13
  (70 shorter events, 13.4 us)
Async XLA Ops:
  6.5 15.9 %copy-start.4 = (bf16[768,512]{1,0:T(8,128)(2,1)S(1)}, bf16[768,512]{1,0:T(8,128)(2,1)}, u32[]{:S(2)}) copy-start(bf16[768,512]{1,0:T(8,128)(2,1)} %param.13) | copy-start | bytes 2359300
  6.5 35.7 %all-gather.6.cloned.1.call-start = ((), (), s32[]{:S(2)}) async-start(), calls=%async_computation.2 | async-start | bytes 2359296 | tf_op jit(solution)/shard_map/all_gather | solution.py:91
  7.3 18.0 %copy-start.12 = (f32[8]{0:T(128)S(1)}, f32[8]{0:T(128)}, u32[]{:S(2)}) copy-start(f32[8]{0:T(128)} %param.17) | copy-start | bytes 100
  7.3 82.4 %reduce-scatter.3.cloned.1.call-start = ((), (), s32[]{:S(2)}) async-start(), calls=%async_computation.3 | async-start | bytes 4718592 | tf_op jit(solution)/shard_map/reduce_scatter | solution.py:92
  8.0 18.4 %collective-permute-start.1 = (s32[128]{0:T(128)S(1)}, s32[128]{0:T(128)S(1)}, u32[]{:S(2)}, u32[]{:S(2)}) collective-permute-start(s32[128]{0:T(128)S(1)} %slice.40), channel_id=1, source_target_pairs={{0,2},{2,4},{4,6},{6,8},{8,10},{10,12},{12,14},{1,3},{3,5},{5,7},{... | collective-permute-start | bytes 1544 | tf_op jit(solution)/shard_map/ppermute | solution.py:15
  11.2 16.2 %collective-permute-start.2 = (bf16[128,256]{1,0:T(8,128)(2,1)S(1)}, bf16[128,256]{1,0:T(8,128)(2,1)}, u32[]{:S(2)}, u32[]{:S(2)}) collective-permute-start(bf16[128,256]{1,0:T(8,128)(2,1)S(1)} %slice.43), channel_id=1, source_target_pairs={{0,2},{2,4},{4,6},{6,8},{8,10},{10,12},{12,14},{1,3},{3,5},{5,7},{... | collective-permute-start | bytes 196616 | tf_op jit(solution)/shard_map/ppermute | solution.py:15
  17.3 12.6 %collective-permute-start = (bf16[128,256]{1,0:T(8,128)(2,1)S(1)}, bf16[128,256]{1,0:T(8,128)(2,1)S(1)}, u32[]{:S(2)}, u32[]{:S(2)}) collective-permute-start(bf16[128,256]{1,0:T(8,128)(2,1)S(1)} %slice.36), channel_id=1, source_target_pairs={{0,2},{2,4},{4,6},{6,8},{8,10},{10,12},{12,14},{1,3},{3,5},{5,7},{... | collective-permute-start | bytes 196616 | tf_op jit(solution)/shard_map/ppermute | solution.py:15
  20.5 5.9 %copy-start.8 = (s32[768]{0:T(1024)S(1)}, s32[768]{0:T(1024)}, u32[]{:S(2)}) copy-start(s32[768]{0:T(1024)} %param.16) | copy-start | bytes 9220
  20.5 6.9 %copy-start = (bf16[768,256]{1,0:T(8,128)(2,1)S(1)}, bf16[768,256]{1,0:T(8,128)(2,1)}, u32[]{:S(2)}) copy-start(bf16[768,256]{1,0:T(8,128)(2,1)} %param.14) | copy-start | bytes 1179652
  24.1 5.7 copy-start.1
  27.4 3.9 copy-start.2
  28.7 2.6 copy-start.6
  33.7 1.8 copy-start.5
  33.7 1.8 copy-start.7
  47.3 44.1 %copy-start.3 = (bf16[384,2048]{1,0:T(8,128)(2,1)S(1)}, bf16[384,2048]{1,0:T(8,128)(2,1)}, u32[]{:S(2)}) copy-start(bf16[384,2048]{1,0:T(8,128)(2,1)} %param.19) | copy-start | bytes 4718596
  47.3 44.1 %copy-start.9 = (f32[2048]{0:T(1024)S(1)}, f32[2048]{0:T(1024)}, u32[]{:S(2)}) copy-start(f32[2048]{0:T(1024)} %param.20) | copy-start | bytes 24580
  47.3 93.4 %all-gather.8.cloned.1.call-start = ((), (), s32[]{:S(2)}) async-start(), calls=%async_computation.4 | async-start | bytes 4718592 | tf_op jit(solution)/shard_map/all_gather | solution.py:106
  91.5 2.7 copy-start.10
  95.7 163.3 %all-gather.10.cloned.1.call-start = ((), (), s32[]{:S(2)}) async-start(), calls=%async_computation.5 | async-start | bytes 14155776 | tf_op jit(solution)/shard_map/all_gather | solution.py:102
  96.3 279.2 %all-gather.12.cloned.1.call-start = ((), (), s32[]{:S(2)}) async-start(), calls=%async_computation.6 | async-start | bytes 14155776 | tf_op jit(solution)/shard_map/all_gather | solution.py:103
  96.9 395.4 %all-gather.14.cloned.1.call-start = ((), (), s32[]{:S(2)}) async-start(), calls=%async_computation.7 | async-start | bytes 14155776 | tf_op jit(solution)/shard_map/all_gather | solution.py:104
  97.4 468.1 %reduce-scatter.5.cloned.1.call-start = ((), (), s32[]{:S(2)}) async-start(), calls=%async_computation.8 | async-start | bytes 4718592 | tf_op jit(solution)/shard_map/reduce_scatter | solution.py:111
  523.8 43.6 %copy-start.11 = (f32[2048]{0:T(1024)S(1)}, f32[2048]{0:T(1024)}, u32[]{:S(2)}) copy-start(f32[2048]{0:T(1024)} %param.22) | copy-start | bytes 24580
Sparse Core Ops, SparseCore 0:
  8.9 33.2 all-gather.5
  47.5 42.1 reduce-scatter.2
  95.8 44.9 all-gather.7
  142.3 116.6 all-gather.9
  260.5 114.8 all-gather.11
  376.9 115.3 all-gather.13
  523.9 41.6 reduce-scatter.4
where the time goes:
time: 578 us
  waiting for transfers between devices  469 us (81%)
  matrix products  56.5 us (10%)
  other arithmetic  15.1 us (3%)
  between operations  13.8 us (2%)
  local copies, waits for them, and re-layouts  13.5 us (2%)
  starting transfers between devices  9.3 us (2%)
    all_gather x1, waiting for transfers between devices, per_device(): lax.all_gather(gate_weight, 'sp', axis=0, tiled=True)  118 us
    all_gather x1, waiting for transfers between devices, per_device(): lax.all_gather(down_weight, 'sp', axis=1, tiled=True)  117 us
    all_gather x1, waiting for transfers between devices, per_device(): lax.all_gather(up_weight, 'sp', axis=0, tiled=True)  100 us
    all_gather x1, waiting for transfers between devices, per_device(): piece = lax.all_gather(normed, 'tp', axis=0, tiled=True)  43.1 us
    reduce_scatter x1, waiting for transfers between devices, per_device(): lax.psum_scatter(jnp.dot(mixed, head_columns, preferred_element_type=jnp....  42.3 us
    reduce_scatter x1, waiting for transfers between devices, per_device(): lax.psum_scatter(jnp.dot(hidden, full_down, preferred_element_type=jnp.fl...  41.8 us
    dot_general x1, matrix products, per_device(): jnp.dot(hidden, full_down, preferred_element_type=jnp.float32)  31.5 us
    dot_general x1, matrix products, per_device(): gate = jnp.dot(piece, full_gate, preferred_element_type=jnp.float32)  16 us
  transfers between devices with their start and end apart: 10, of which 7 were waited for; matrix products, arithmetic and copies ran while one was open for 6% of the time, Pallas kernels for 0%

commit v1 on v0

--- a/solution.py
+++ b/solution.py
@@ -101,7 +101,7 @@
     full_gate, full_up, full_down = (
         lax.all_gather(gate_weight, "sp", axis=0, tiled=True),
         lax.all_gather(up_weight, "sp", axis=0, tiled=True),
-        lax.all_gather(down_weight, "sp", axis=1, tiled=True),
+        jnp.concatenate(lax.all_gather(down_weight, "sp"), axis=1),
     )
     piece = lax.all_gather(normed, "tp", axis=0, tiled=True)
     gate = jnp.dot(piece, full_gate, preferred_element_type=jnp.float32)

time: 578 us -> 571 us (0.988)
  waiting for transfers between devices: 469 us -> 452 us
  local copies, waits for them, and re-layouts: 13.5 us -> 26.8 us
    reshape x0 -> x1, local copies, waits for them, and re-layouts: none -> 15.9 us  [per_device(): jnp.concatenate(lax.all_gather(down_weight, 'sp'), axis=1)]
    all_gather x1, waiting for transfers between devices: 43.1 us -> 28.6 us  [per_device(): piece = lax.all_gather(normed, 'tp', axis=0, tiled=True)]
  transfers between devices with their start and end apart: 10 -> 10, of which waited for: 7 -> 7; matrix products, arithmetic and copies ran while one was open for 6% -> 10% of each run, Pallas kernels for 0% -> 0%
where the time goes in v1:
time: 571 us; the launch traced here: 570 us
  waiting for transfers between devices  452 us (79%)
  matrix products  54.4 us (10%)
  local copies, waits for them, and re-layouts  26.8 us (5%)
  other arithmetic  14.1 us (2%)
  between operations  13.8 us (2%)
  starting transfers between devices  9.28 us (2%)
    all_gather x1, waiting for transfers between devices, per_device(): lax.all_gather(gate_weight, 'sp', axis=0, tiled=True)  118 us
    all_gather x1, waiting for transfers between devices, per_device(): lax.all_gather(down_weight, 'sp')  111 us
    all_gather x1, waiting for transfers between devices, per_device(): lax.all_gather(up_weight, 'sp', axis=0, tiled=True)  100 us
    reduce_scatter x1, waiting for transfers between devices, per_device(): lax.psum_scatter(jnp.dot(hidden, full_down, preferred_element_type=jnp.fl...  41.8 us
    reduce_scatter x1, waiting for transfers between devices, per_device(): lax.psum_scatter(jnp.dot(mixed, head_columns, preferred_element_type=jnp....  41.3 us
    dot_general x1, matrix products, per_device(): jnp.dot(hidden, full_down, preferred_element_type=jnp.float32)  29.1 us
    all_gather x1, waiting for transfers between devices, per_device(): piece = lax.all_gather(normed, 'tp', axis=0, tiled=True)  28.6 us
    dot_general x1, matrix products, per_device(): gate = jnp.dot(piece, full_gate, preferred_element_type=jnp.float32)  15.9 us
  transfers between devices with their start and end apart: 10, of which 7 were waited for; matrix products, arithmetic and copies ran while one was open for 10% of the time, Pallas kernels for 0%

profile of v1, /device:TPU:0, one launch (start us, length us, event | category | flops | bytes accessed | tf_op | source)
XLA Modules:
  0.0 570.2 jit_solution(3396466697669586101)
XLA Ops:
  8.0 2.4 collective-permute-start.1
  11.2 4.6 collective-permute-start.2
  16.7 1.9 collective-permute-start
  18.7 1.8 reshape.116
  20.5 1.9 reshape.114
  22.4 1.7 reshape.117
  27.9 2.7 fusion.2
  30.6 1.7 fusion
  32.4 1.6 fusion.20
  34.6 7.6 %all-gather.7.cloned.1.call-done = bf16[512,2048]{1,0:T(8,128)(2,1)} async-done(((bf16[512,256]{1,0:T(8,128)(2,1)}), bf16[512,2048]{1,0:T(8,128)(2,1)}) %all-gather.7.cloned.1.call-update) | async-done | bytes 2097168 | tf_op jit(solution)/shard_map/all_gather | solution.py:91
  42.2 5.1 convolution_convert_fusion
  48.3 41.3 %reduce-scatter.3.cloned.1.call-done = bf16[384,2048]{1,0:T(8,128)(2,1)} async-done(((bf16[768,2048]{1,0:T(8,128)(2,1)}), bf16[384,2048]{1,0:T(8,128)(2,1)}) %reduce-scatter.3.cloned.1.call-update) | async-done | bytes 1572880 | tf_op jit(solution)/shard_map/reduce_scatter | solution.py:92
  89.6 1.8 fusion.3
  91.5 2.2 fusion.6
  96.9 111.1 %all-gather.15.cloned.1.call-done = bf16[24576,256]{1,0:T(8,128)(2,1)} async-done(((bf16[3072,256]{1,0:T(8,128)(2,1)}), bf16[24576,256]{1,0:T(8,128)(2,1)}) %all-gather.15.cloned.1.call-update) | async-done | bytes 12582928 | tf_op jit(solution)/shard_map/all_gather | solution.py:104
  208.0 15.9 %copy.40 = bf16[3072,8,256]{0,2,1:T(8,128)(2,1)} copy(bf16[3072,8,256]{2,0,1:T(8,128)(2,1)} %bitcast.49) | data formatting | bytes 25165824 | tf_op jit(solution)/shard_map/reshape | solution.py:104
  223.9 28.6 %all-gather.9.cloned.1.call-done = bf16[768,2048]{1,0:T(8,128)(2,1)} async-done(((bf16[384,2048]{1,0:T(8,128)(2,1)}), bf16[768,2048]{1,0:T(8,128)(2,1)}) %all-gather.9.cloned.1.call-update) | async-done | bytes 3145744 | tf_op jit(solution)/shard_map/all_gather | solution.py:106
  252.6 118.2 %all-gather.11.cloned.1.call-done = bf16[2048,3072]{1,0:T(8,128)(2,1)} async-done(((bf16[256,3072]{1,0:T(8,128)(2,1)}), bf16[2048,3072]{1,0:T(8,128)(2,1)}) %all-gather.11.cloned.1.call-update) | async-done | bytes 12582928 | tf_op jit(solution)/shard_map/all_gather | solution.py:102
  370.8 15.9 %fusion.40 = f32[768,3072]{1,0:T(8,128)} fusion(bf16[768,2048]{1,0:T(8,128)(2,1)} %all-gather.9.cloned.1.call-done, bf16[2048,3072]{1,0:T(8,128)(2,1)} %all-gather.11.cloned.1.call-done), kind=kOutput, calls=%fused_computation.68 | convolution fusion | flops 9663676416 | bytes 25165824 | tf_op jit(solution)/shard_map/dot_general | solution.py:107
  386.7 100.5 %all-gather.13.cloned.1.call-done = bf16[2048,3072]{1,0:T(8,128)(2,1)} async-done(((bf16[256,3072]{1,0:T(8,128)(2,1)}), bf16[2048,3072]{1,0:T(8,128)(2,1)}) %all-gather.13.cloned.1.call-update) | async-done | bytes 12582928 | tf_op jit(solution)/shard_map/all_gather | solution.py:103
  487.2 29.1 %convolution_convert_fusion.1 = bf16[768,2048]{1,0:T(8,128)(2,1)} fusion(bf16[3072,2048]{0,1:T(8,128)(2,1)} %bitcast.50, f32[768,3072]{1,0:T(8,128)} %fusion.40, bf16[768,2048]{1,0:T(8,128)(2,1)} %all-gather.9.cloned.1.call-done, bf16[2048,3072]{1,0:T(8,128)(2,1)} %all-gather.13.cloned.1.call-done), kind=kOutput, calls=%fused_computation.14 | convolution fusion | flops 19343081472 | bytes 40894464 | tf_op jit(solution)/shard_map/dot_general | solution.py:112
  516.4 41.8 %reduce-scatter.5.cloned.1.call-done = bf16[384,2048]{1,0:T(8,128)(2,1)} async-done(((bf16[768,2048]{1,0:T(8,128)(2,1)}), bf16[384,2048]{1,0:T(8,128)(2,1)}) %reduce-scatter.5.cloned.1.call-update) | async-done | bytes 1572880 | tf_op jit(solution)/shard_map/reduce_scatter | solution.py:111
  558.1 1.8 fusion.7
  560.0 3.4 fusion.13
  (63 shorter events, 11.6 us)
Async XLA Ops:
  6.5 15.9 %copy-start.3 = (bf16[768,512]{1,0:T(8,128)(2,1)S(1)}, bf16[768,512]{1,0:T(8,128)(2,1)}, u32[]{:S(2)}) copy-start(bf16[768,512]{1,0:T(8,128)(2,1)} %param.13) | copy-start | bytes 2359300
  6.5 35.7 %all-gather.7.cloned.1.call-start = ((), (), s32[]{:S(2)}) async-start(), calls=%async_computation.2 | async-start | bytes 2359296 | tf_op jit(solution)/shard_map/all_gather | solution.py:91
  7.3 17.3 %copy-start.8 = (f32[8]{0:T(128)S(1)}, f32[8]{0:T(128)}, u32[]{:S(2)}) copy-start(f32[8]{0:T(128)} %param.17) | copy-start | bytes 100
  7.3 82.4 %reduce-scatter.3.cloned.1.call-start = ((), (), s32[]{:S(2)}) async-start(), calls=%async_computation.3 | async-start | bytes 4718592 | tf_op jit(solution)/shard_map/reduce_scatter | solution.py:92
  8.0 17.1 %collective-permute-start.1 = (s32[128]{0:T(128)S(1)}, s32[128]{0:T(128)S(1)}, u32[]{:S(2)}, u32[]{:S(2)}) collective-permute-start(s32[128]{0:T(128)S(1)} %slice.40), channel_id=1, source_target_pairs={{0,2},{2,4},{4,6},{6,8},{8,10},{10,12},{12,14},{1,3},{3,5},{5,7},{... | collective-permute-start | bytes 1544 | tf_op jit(solution)/shard_map/ppermute | solution.py:15
  11.2 14.9 %collective-permute-start.2 = (bf16[128,256]{1,0:T(8,128)(2,1)S(1)}, bf16[128,256]{1,0:T(8,128)(2,1)S(1)}, u32[]{:S(2)}, u32[]{:S(2)}) collective-permute-start(bf16[128,256]{1,0:T(8,128)(2,1)S(1)} %slice.43), channel_id=1, source_target_pairs={{0,2},{2,4},{4,6},{6,8},{8,10},{10,12},{12,14},{1,3},{3,5},{5,7},{... | collective-permute-start | bytes 196616 | tf_op jit(solution)/shard_map/ppermute | solution.py:15
  16.7 10.3 %collective-permute-start = (bf16[128,256]{1,0:T(8,128)(2,1)S(1)}, bf16[128,256]{1,0:T(8,128)(2,1)S(1)}, u32[]{:S(2)}, u32[]{:S(2)}) collective-permute-start(bf16[128,256]{1,0:T(8,128)(2,1)S(1)} %slice.36), channel_id=1, source_target_pairs={{0,2},{2,4},{4,6},{6,8},{8,10},{10,12},{12,14},{1,3},{3,5},{5,7},{... | collective-permute-start | bytes 196616 | tf_op jit(solution)/shard_map/ppermute | solution.py:15
  20.5 4.7 copy-start.4
  20.5 5.7 copy-start
  24.1 2.9 copy-start.1
  47.3 44.1 %copy-start.2 = (bf16[384,2048]{1,0:T(8,128)(2,1)S(1)}, bf16[384,2048]{1,0:T(8,128)(2,1)}, u32[]{:S(2)}) copy-start(bf16[384,2048]{1,0:T(8,128)(2,1)} %param.19) | copy-start | bytes 4718596
  47.3 44.1 %copy-start.5 = (f32[2048]{0:T(1024)S(1)}, f32[2048]{0:T(1024)}, u32[]{:S(2)}) copy-start(f32[2048]{0:T(1024)} %param.20) | copy-start | bytes 24580
  47.3 160.7 %all-gather.15.cloned.1.call-start = ((), (), s32[]{:S(2)}) async-start(), calls=%async_computation.8 | async-start | bytes 14155776 | tf_op jit(solution)/shard_map/all_gather | solution.py:104
  48.1 204.5 %all-gather.9.cloned.1.call-start = ((), (), s32[]{:S(2)}) async-start(), calls=%async_computation.4 | async-start | bytes 4718592 | tf_op jit(solution)/shard_map/all_gather | solution.py:106
  91.5 2.7 copy-start.6
  95.7 275.1 %all-gather.11.cloned.1.call-start = ((), (), s32[]{:S(2)}) async-start(), calls=%async_computation.5 | async-start | bytes 14155776 | tf_op jit(solution)/shard_map/all_gather | solution.py:102
  96.3 390.9 %all-gather.13.cloned.1.call-start = ((), (), s32[]{:S(2)}) async-start(), calls=%async_computation.6 | async-start | bytes 14155776 | tf_op jit(solution)/shard_map/all_gather | solution.py:103
  96.9 461.3 %reduce-scatter.5.cloned.1.call-start = ((), (), s32[]{:S(2)}) async-start(), calls=%async_computation.7 | async-start | bytes 4718592 | tf_op jit(solution)/shard_map/reduce_scatter | solution.py:111
  516.3 43.6 %copy-start.7 = (f32[2048]{0:T(1024)S(1)}, f32[2048]{0:T(1024)}, u32[]{:S(2)}) copy-start(f32[2048]{0:T(1024)} %param.22) | copy-start | bytes 24580
Sparse Core Ops, SparseCore 0:
  8.9 33.2 all-gather.6
  47.5 42.1 reduce-scatter.2
  91.3 116.7 all-gather.14
  209.4 43.0 all-gather.8
  254.1 116.6 all-gather.10
  372.3 114.8 all-gather.12
  516.5 41.6 reduce-scatter.4
